TPU v7x, 32 devices: a whole 2x2x4 slice. The times are simulated.
32 devices in a mesh: sp: 4 (over z), fs: 4 (over y, x), tp: 2 (over core).
Axes of the slice: x: 2, y: 2, z: 4, core: 2. Of those that a mesh axis runs over, the one named last changes fastest.
Arguments:
- inputs: bfloat16 [4, 2048, 2048], P('fs', 'sp', 'tp'), may hold values from -6 to 6
- norm_gain: float32 [2048], replicated, may hold values from 0.1 to 1.9
- query_weight: bfloat16 [2048, 1024], P(('sp', 'fs'), 'tp'), may hold values from -0.125 to 0.125
- key_weight: bfloat16 [2048, 1024], P(('sp', 'fs'), 'tp'), may hold values from -0.125 to 0.125
- value_weight: bfloat16 [2048, 1024], P(('sp', 'fs'), 'tp'), may hold values from -0.125 to 0.125
- query_gain: float32 [64], replicated, may hold values from 0.8 to 7
- key_gain: float32 [64], replicated, may hold values from 0.8 to 7
- mix_lambda: float32 [8], replicated, may hold values from 0.3 to 0.8
- head_gain: float32 [128], replicated, may hold values from 0.1 to 1.9
- post_gate_weight: bfloat16 [2048, 2048], P(('sp', 'fs'), 'tp'), may hold values from -0.125 to 0.125
- pre_gate_weight: bfloat16 [2048, 2048], P(('sp', 'fs'), 'tp'), may hold values from -0.125 to 0.125
- inner_weight: bfloat16 [2048, 2048], P(('sp', 'fs'), 'tp'), may hold values from -0.125 to 0.125
- conv_taps: float32 [3, 2048], replicated, may hold values from -3 to 3
- attn_out_weight: bfloat16 [2048, 1024], P(('sp', 'fs'), 'tp'), may hold values from -0.109375 to 0.109375
- conv_out_weight: bfloat16 [2048, 2048], P(('sp', 'fs'), 'tp'), may hold values from -0.109375 to 0.109375
Outputs:
- mixed: bfloat16 [4, 2048, 2048], P('fs', ('sp', 'tp'))
All inputs are finite; a program needn't handle non-finite values.
Results may differ from a plain program's by a relative error of at most 0.015.
The roundings to bfloat16 on the way count: a program that leaves them out, or rounds other values in their place, can miss the bound.
Values may be sent and summed in bfloat16 or wider, within the bound.
A program may use at most 128 MiB of HBM per device.

v0:
```python
import math

import jax
import jax.numpy as jnp
from jax import lax
from jax.experimental import pallas as pl
from jax.experimental.pallas import tpu as pltpu
from jax.sharding import PartitionSpec as P

epsilon = 1e-06


def padded_2(x, sides, width):
    for axis, dim in sides:
        size, length = (lax.axis_size(axis), x.shape[dim])
        up = [(i, (i + 1) % size) for i in range(size - 1)]
        down = [(j, i) for i, j in up]
        last = lax.slice_in_dim(x, length - width, length, axis=dim)
        initial = lax.slice_in_dim(x, 0, width, axis=dim)
        before = lax.ppermute(last, axis, up)
        after = lax.ppermute(initial, axis, down)
        x = jnp.concatenate([before, x, after], axis=dim)
    return x


def scale_rows(values, gain):
    return values * lax.rsqrt(jnp.mean(values * values, axis=-1, keepdims=True) + epsilon) * gain


def project_all(normed, weights, products):
    result = []
    for member in range(len(weights)):
        if member < products:
            result.append(jnp.dot(normed, weights[member], preferred_element_type=jnp.float32))
        else:
            result.append(weights[member])
    return tuple(result)


def attention_branch(query, key, values, weight_two, query_gain, key_gain, head_gain):
    tok_rows = query.shape[0]
    vsize = head_gain.shape[0]
    half = query_gain.shape[0]
    heads = values.shape[1] // vsize
    query_normed = scale_rows(query.reshape(tok_rows, heads, 2, half), query_gain).astype(
        jnp.bfloat16
    )
    key_normed = scale_rows(key.reshape(tok_rows, heads * 2, half), key_gain).astype(jnp.bfloat16)
    key_normed = key_normed.reshape(tok_rows, heads * 2 * half)
    scale = half ** (-0.5)
    initial = (
        jnp.full((heads, 2, tok_rows), -1e30, jnp.float32),
        jnp.zeros((heads, 2, tok_rows), jnp.float32),
        jnp.zeros((heads, 2, tok_rows, vsize), jnp.float32),
    )
    carry = initial
    key_piece = lax.all_gather(key_normed, "sp", axis=0, tiled=True)
    value_piece = lax.all_gather(values, "sp", axis=0, tiled=True)
    length = key_piece.shape[0]
    block = math.gcd(length, 512)
    key_blocks = key_piece.reshape(length // block, block, heads, 2, half)
    value_blocks = value_piece.reshape(length // block, block, heads, vsize)

    def one_block(state, blocks):
        peak, total, accum = state
        key_block, value_block = blocks
        scores = (
            jnp.einsum(
                "qhjd,khjd->hjqk", query_normed, key_block, preferred_element_type=jnp.float32
            )
            * scale
        )
        new_peak = jnp.maximum(peak, jnp.max(scores, axis=-1))
        factor = jnp.exp(peak - new_peak)
        expo = jnp.exp(scores - new_peak[..., None])
        total = total * factor + jnp.sum(expo, axis=-1)
        accum = accum * factor[..., None] + jnp.einsum(
            "hjqk,khd->hjqd",
            expo.astype(jnp.bfloat16),
            value_block,
            preferred_element_type=jnp.float32,
        )
        return ((new_peak, total, accum), None)

    carry, unused = lax.scan(one_block, carry, (key_blocks, value_blocks))
    peak, total, accum = carry
    mapped = accum / total[..., None]
    head_out = mapped[:, 0] - weight_two[:, None, None] * mapped[:, 1]
    normed_out = scale_rows(head_out, head_gain).astype(jnp.bfloat16)
    return jnp.transpose(normed_out, (1, 0, 2)).reshape(tok_rows, heads * vsize)


def half_scaled(values, gain, half):
    low = lax.broadcasted_iota(jnp.int32, (1, 2 * half), 1) < half
    squares = values * values
    first = jnp.sum(jnp.where(low, squares, 0.0), axis=-1, keepdims=True) / half
    second = jnp.sum(jnp.where(low, 0.0, squares), axis=-1, keepdims=True) / half
    factor = jnp.where(low, lax.rsqrt(first + epsilon), lax.rsqrt(second + epsilon))
    return values * factor * gain


def attention_kernel(half, q_ref, k_ref, v_ref, qg_ref, kg_ref, lam_ref, hg_ref, out_ref, key, val):
    @pl.when(pl.program_id(1) == 0)
    def _():
        key[...] = half_scaled(k_ref[...], kg_ref[...], half).astype(jnp.bfloat16)
        val[...] = v_ref[...].astype(jnp.bfloat16)

    low = lax.broadcasted_iota(jnp.int32, (1, 2 * half), 1) < half
    query = half_scaled(q_ref[...], qg_ref[...], half).astype(jnp.bfloat16).astype(jnp.float32)
    maps = []
    for which in range(2):
        keep = low if which == 0 else jnp.logical_not(low)
        part = jnp.where(keep, query, 0.0).astype(jnp.bfloat16)
        scores = lax.dot_general(
            part, key[...], (((1,), (1,)), ((), ())), preferred_element_type=jnp.float32
        ) * half ** (-0.5)
        expo = jnp.exp(scores - jnp.max(scores, axis=-1, keepdims=True))
        total = jnp.sum(expo, axis=-1, keepdims=True)
        maps.append(
            jnp.dot(expo.astype(jnp.bfloat16), val[...], preferred_element_type=jnp.float32) / total
        )
    head_out = maps[0] - lam_ref[0] * maps[1]
    out_ref[...] = scale_rows(head_out, hg_ref[...]).astype(jnp.bfloat16)


def attention_call(y, heads, query_gain, key_gain, weight_two, head_gain):
    rows = y.shape[0]
    half, vsize = query_gain.shape[0], head_gain.shape[0]
    block = math.gcd(rows, 256)
    small = lambda h, i: (0, 0)
    return pl.pallas_call(
        lambda *refs: attention_kernel(half, *refs),
        out_shape=jax.ShapeDtypeStruct((rows, heads * vsize), jnp.bfloat16),
        grid=(heads, rows // block),
        in_specs=[
            pl.BlockSpec((block, 2 * half), lambda h, i: (i, h)),
            pl.BlockSpec((rows, 2 * half), lambda h, i: (0, heads + h)),
            pl.BlockSpec((rows, vsize), lambda h, i: (0, 2 * heads + h)),
            pl.BlockSpec((1, 2 * half), small),
            pl.BlockSpec((1, 2 * half), small),
            pl.BlockSpec((1, 1, vsize), lambda h, i: (h, 0, 0)),
            pl.BlockSpec((1, vsize), small),
        ],
        out_specs=pl.BlockSpec((block, vsize), lambda h, i: (i, h)),
        scratch_shapes=[
            pltpu.VMEM((rows, 2 * half), jnp.bfloat16),
            pltpu.VMEM((rows, vsize), jnp.bfloat16),
        ],
        compiler_params=pltpu.CompilerParams(vmem_limit_bytes=40 * 2**20),
        cost_estimate=pl.CostEstimate(
            flops=heads * rows * rows * 8 * half * 2,
            bytes_accessed=rows * heads * vsize * 14,
            transcendentals=2 * heads * rows * rows,
        ),
    )(
        y,
        y,
        y,
        jnp.tile(query_gain, 2)[None],
        jnp.tile(key_gain, 2)[None],
        jnp.broadcast_to(weight_two[:, None, None], (heads, 1, vsize)),
        head_gain[None],
    )


def column_parts(weights, parts):
    rows = weights[0].shape[0]
    pieces = [w.reshape(rows, parts, w.shape[1] // parts) for w in weights]
    return jnp.transpose(jnp.concatenate(pieces, axis=2), (1, 0, 2))


def remote(source, target, send, recv, where):
    return pltpu.make_async_remote_copy(
        src_ref=source,
        dst_ref=target,
        send_sem=send,
        recv_sem=recv,
        device_id=where,
        device_id_type=pl.DeviceIdType.MESH,
    )


def meet(places):
    barrier = pltpu.get_barrier_semaphore()
    for where in places:
        pl.semaphore_signal(
            barrier, inc=1, device_id=where, device_id_type=pl.DeviceIdType.MESH
        )
    pl.semaphore_wait(barrier, len(places))


def gather_kernel(
    n, w_ref, t_ref, w_all, t_all, own, z_send, z_recv, f_send, f_recv, g_send, g_recv,
    t_send, t_recv, p_send, p_recv,
):
    z, f, c = lax.axis_index("sp"), lax.axis_index("fs"), lax.axis_index("tp")
    beside, above = f + 1 - 2 * (f % 2), f + 2 - 4 * (f // 2)
    rows = t_ref.shape[0]
    near = sorted(range(1, n), key=lambda d: min(d, n - d))
    meet(
        [{"sp": (z + d) % n} for d in near] + [{"fs": beside}, {"fs": above}, {"tp": 1 - c}]
    )

    def place(s):
        return t_all.at[c, pl.ds(pl.multiple_of(s * rows, rows), rows)]

    flights = []

    def go(copy):
        copy.start()
        flights.append(copy)
        return copy

    across = {
        d: go(
            remote(
                w_ref.at[(z + d) % n], w_all.at[z, f], z_send.at[d], z_recv.at[d], {"sp": (z + d) % n}
            )
        )
        for d in near
    }
    side = {}

    def spread(d, source):
        s = (z + n - d) % n
        for i, to in enumerate((beside, above)):
            side[i, d] = go(
                remote(source, w_all.at[s, f], f_send.at[i, d], f_recv.at[i, d], {"fs": to})
            )

    def pass_on(d):
        s = (z + n - d) % n
        i = d % 2
        side[i, d].wait_recv()
        held, to = (beside, above) if i == 0 else (above, beside)
        go(remote(w_all.at[s, held], w_all.at[s, held], g_send.at[d], g_recv.at[d], {"fs": to}))

    spread(0, w_ref.at[z])
    def along(source, s, step):
        return remote(source, place(s), t_send.at[(step + 1) // 2, s], t_recv.at[s], {"sp": z + step})

    def aside(source, s):
        return remote(source, place(s), p_send.at[s], p_recv.at[s], {"tp": 1 - c})

    @pl.when(z + 1 < n)
    def _():
        along(t_ref, z, 1).start()

    @pl.when(z > 0)
    def _():
        along(t_ref, z, -1).start()

    aside(t_ref, z).start()
    mine = [
        pltpu.make_async_copy(w_ref.at[z], w_all.at[z, f], own.at[0]),
        pltpu.make_async_copy(t_ref, place(z), own.at[1]),
    ]
    for copy in mine:
        copy.start()
    last = 0
    for d in near:
        across[d].wait_recv()
        spread(d, w_all.at[(z + n - d) % n, f])
        pass_on(last)
        last = d
    pass_on(last)
    for k in range(1, n):
        for step in (1, -1):
            s = z - step * k

            @pl.when(jnp.logical_and(s >= 0, s < n))
            def _(s=s, step=step):
                along(place(s), s, step).wait_recv()

                @pl.when(jnp.logical_and(z + step >= 0, z + step < n))
                def _():
                    along(place(s), s, step).start()

                aside(place(s), s).start()

    for k in range(n):
        for step in (1, -1) if k else (1,):
            s = z - step * k

            @pl.when(jnp.logical_and(s >= 0, s < n))
            def _(s=s, step=step, k=k):
                for way in (step,) if k else (1, -1):
                    @pl.when(jnp.logical_and(z + way >= 0, z + way < n))
                    def _(way=way):
                        along(place(s), s, way).wait_send()

                aside(place(s), s).wait_send()
                aside(place(s), s).wait_recv()

    waited = set(map(id, across.values()))
    waited |= {id(side[d % 2, d]) for d in range(n)}
    for copy in flights:
        copy.wait_send()
        if id(copy) not in waited:
            copy.wait_recv()
    for copy in mine:
        copy.wait()


def gather_all(packed, tokens):
    n, rows, columns = packed.shape
    fs, tp = lax.axis_size("fs"), lax.axis_size("tp")
    dma = pltpu.SemaphoreType.DMA
    return pl.pallas_call(
        lambda *refs: gather_kernel(n, *refs),
        out_shape=(
            jax.ShapeDtypeStruct((n, fs, rows, columns), packed.dtype),
            jax.ShapeDtypeStruct((tp, n * tokens.shape[0], tokens.shape[1]), tokens.dtype),
        ),
        in_specs=[pl.BlockSpec(memory_space=pltpu.VMEM)] * 2,
        out_specs=(pl.BlockSpec(memory_space=pl.ANY),) * 2,
        scratch_shapes=[
            dma((2,)), dma((n,)), dma((n,)), dma((2, n)), dma((2, n)), dma((n,)), dma((n,)),
            dma((2, n)), dma((n,)), dma((n,)), dma((n,)),
        ],
        compiler_params=pltpu.CompilerParams(collective_id=1, has_side_effects=True),
    )(packed, tokens)


def reduce_kernel(n, p_ref, out_ref, twin, pair, others, a_send, a_recv, b_send, b_recv):
    z, c = lax.axis_index("sp"), lax.axis_index("tp")
    near = sorted(range(1, n), key=lambda d: -min(d, n - d))
    meet([{"sp": (z + d) % n} for d in near] + [{"tp": 1 - c}])
    rows = out_ref.shape[0]
    tile = math.gcd(rows, 32)
    swaps = {}
    for d in near + [0]:
        s = (z + d) % n
        swaps[d] = remote(
            p_ref.at[1 - c, s], twin.at[d], a_send.at[d], a_recv.at[d], {"tp": 1 - c}
        )
        swaps[d].start()
    sends = {}
    for d in near + [0]:
        s = (z + d) % n
        swaps[d].wait_recv()

        def add(i, unused, s=s, d=d):
            at = pl.ds(pl.multiple_of(i * tile, tile), tile)
            total = p_ref[c, s, at, :].astype(jnp.float32) + twin[d, at, :].astype(jnp.float32)
            pair[d, at, :] = total.astype(jnp.bfloat16)
            return unused

        lax.fori_loop(0, rows // tile, add, 0)
        if d:
            sends[d] = remote(
                pair.at[d], others.at[d - 1], b_send.at[d - 1], b_recv.at[d - 1], {"sp": s}
            )
            sends[d].start()
    for d in near:
        sends[d].wait_recv()

    def finish(i, unused):
        at = pl.ds(pl.multiple_of(i * tile, tile), tile)
        total = pair[0, at, :].astype(jnp.float32)
        for d in range(1, n):
            total += others[d - 1, at, :].astype(jnp.float32)
        out_ref[at, :] = total.astype(jnp.bfloat16)
        return unused

    lax.fori_loop(0, rows // tile, finish, 0)
    for d in near + [0]:
        swaps[d].wait_send()
    for d in near:
        sends[d].wait_send()


def reduce_all(partial):
    tp, n, rows, width = partial.shape
    dma = pltpu.SemaphoreType.DMA
    return pl.pallas_call(
        lambda *refs: reduce_kernel(n, *refs),
        out_shape=jax.ShapeDtypeStruct((rows, width), partial.dtype),
        in_specs=[pl.BlockSpec(memory_space=pltpu.VMEM)],
        out_specs=pl.BlockSpec(memory_space=pltpu.VMEM),
        scratch_shapes=[
            pltpu.VMEM((n, rows, width), partial.dtype),
            pltpu.VMEM((n, rows, width), partial.dtype),
            pltpu.VMEM((n - 1, rows, width), partial.dtype),
            dma((n,)), dma((n,)), dma((n - 1,)), dma((n - 1,)),
        ],
        compiler_params=pltpu.CompilerParams(
            collective_id=2, has_side_effects=True, vmem_limit_bytes=48 * 2**20
        ),
    )(partial)


def split_device(
    inputs,
    norm_gain,
    query_weight,
    key_weight,
    value_weight,
    query_gain,
    key_gain,
    mix_lambda,
    head_gain,
    post_gate_weight,
    pre_gate_weight,
    inner_weight,
    conv_taps,
    attn_out_weight,
    conv_out_weight,
):
    sp, tp = lax.axis_size("sp"), lax.axis_size("tp")
    tokens = inputs[0]
    place = lax.axis_index("tp") * sp + lax.axis_index("sp")
    vsize = head_gain.shape[0]
    heads = value_weight.shape[1] // vsize // sp
    channels = post_gate_weight.shape[1] // sp
    weight_two = lax.dynamic_slice_in_dim(mix_lambda, place * heads, heads)
    taps = lax.dynamic_slice_in_dim(conv_taps, place * channels, channels, 1)
    packed = column_parts(
        (
            query_weight,
            key_weight,
            value_weight,
            post_gate_weight,
            pre_gate_weight,
            inner_weight,
            attn_out_weight,
            conv_out_weight,
        ),
        sp,
    )
    every, both = gather_all(packed, tokens)
    every = every.reshape(-1, packed.shape[2])
    cut = 3 * heads * vsize + 3 * channels
    into, outof = every[:, :cut], every[:, cut:]
    whole = jnp.concatenate([both[i] for i in range(tp)], axis=1)
    normed = scale_rows(whole.astype(jnp.float32), norm_gain).astype(jnp.bfloat16)
    y = jnp.dot(normed, into, preferred_element_type=jnp.float32)
    attn_hidden = attention_call(y, heads, query_gain, key_gain, weight_two, head_gain)
    span = 3 * heads * vsize
    post, pre_gate, inner = [
        y[:, span + i * channels : span + (i + 1) * channels] for i in range(3)
    ]
    post_wide = lax.optimization_barrier(post.astype(jnp.bfloat16)).astype(jnp.float32)
    signal = lax.optimization_barrier((pre_gate * inner).astype(jnp.bfloat16))
    shifted = jnp.pad(signal.astype(jnp.float32), ((1, 1), (0, 0)))
    filtered = taps[0] * shifted[:-2] + taps[1] * shifted[1:-1] + taps[2] * shifted[2:]
    conv_hidden = (post_wide * filtered).astype(jnp.bfloat16)
    hidden = jnp.concatenate([attn_hidden, conv_hidden], axis=1)
    width = hidden.shape[1]
    hidden = hidden.reshape(sp, tp, -1, width).transpose(1, 0, 2, 3).reshape(-1, width)
    partial = lax.dot_general(
        hidden, outof, (((1,), (1,)), ((), ())), preferred_element_type=jnp.float32
    ).astype(jnp.bfloat16)
    summed = reduce_all(partial.reshape(tp, sp, -1, partial.shape[1]))
    return summed[None]


def per_device(
    inputs,
    norm_gain,
    query_weight,
    key_weight,
    value_weight,
    query_gain,
    key_gain,
    mix_lambda,
    head_gain,
    post_gate_weight,
    pre_gate_weight,
    inner_weight,
    conv_taps,
    attn_out_weight,
    conv_out_weight,
):
    tokens = inputs[0]
    whole = lax.all_gather(tokens, "tp", axis=1, tiled=True)
    normed = scale_rows(whole.astype(jnp.float32), norm_gain).astype(jnp.bfloat16)
    heads_dev = value_weight.shape[1] // head_gain.shape[0]
    channels = post_gate_weight.shape[1]
    tp_index = lax.axis_index("tp")
    weight_two = lax.dynamic_slice_in_dim(mix_lambda, tp_index * heads_dev, heads_dev)
    taps = lax.dynamic_slice_in_dim(conv_taps, tp_index * channels, channels, 1)
    every_full = (
        lax.all_gather(query_weight, ("sp", "fs"), axis=0, tiled=True),
        lax.all_gather(key_weight, ("sp", "fs"), axis=0, tiled=True),
        lax.all_gather(value_weight, ("sp", "fs"), axis=0, tiled=True),
        lax.all_gather(post_gate_weight, ("sp", "fs"), axis=0, tiled=True),
        lax.all_gather(pre_gate_weight, ("sp", "fs"), axis=0, tiled=True),
        lax.all_gather(inner_weight, ("sp", "fs"), axis=0, tiled=True),
        lax.all_gather(attn_out_weight, ("sp", "fs"), axis=0, tiled=True),
        lax.all_gather(conv_out_weight, ("sp", "fs"), axis=0, tiled=True),
    )
    query, key, value_proj, post, pre_gate, inner, attn_out_full, conv_out_full = project_all(
        normed, every_full[0:3] + every_full[3:6] + every_full[6:8], 6
    )
    attn_hidden = attention_branch(
        query, key, value_proj.astype(jnp.bfloat16), weight_two, query_gain, key_gain, head_gain
    )
    post_mid = post.astype(jnp.bfloat16)
    post_wide = lax.optimization_barrier(post_mid).astype(jnp.float32)
    signal = (pre_gate * inner).astype(jnp.bfloat16)
    padded = padded_2(signal, (("sp", 0),), 1)
    shifted = lax.optimization_barrier(padded).astype(jnp.float32)
    filtered = taps[0] * shifted[:-2] + taps[1] * shifted[1:-1] + taps[2] * shifted[2:]
    conv_hidden = (post_wide * filtered).astype(jnp.bfloat16)
    contract = (((1,), (1,)), ((), ()))
    summed = lax.psum_scatter(
        (
            lax.dot_general(
                attn_hidden, attn_out_full, contract, preferred_element_type=jnp.float32
            )
            + lax.dot_general(
                conv_hidden, conv_out_full, contract, preferred_element_type=jnp.float32
            )
        ).astype(jnp.bfloat16),
        "tp",
        scatter_dimension=0,
        tiled=True,
    )
    return summed[None]


def solution(mesh):
    placed = (
        P("fs", "sp", "tp"),
        P(),
        P(("sp", "fs"), "tp"),
        P(("sp", "fs"), "tp"),
        P(("sp", "fs"), "tp"),
        P(),
        P(),
        P(),
        P(),
        P(("sp", "fs"), "tp"),
        P(("sp", "fs"), "tp"),
        P(("sp", "fs"), "tp"),
        P(),
        P(("sp", "fs"), "tp"),
        P(("sp", "fs"), "tp"),
    )
    sp, tp = mesh.shape["sp"], mesh.shape["tp"]

    def program(*args):
        heads = args[7].shape[0]
        channels = args[12].shape[1]
        splits = tp == 2 and mesh.shape["fs"] == 4 and sp > 1 and heads % (sp * tp) == 0
        splits = splits and channels % (sp * tp * 128) == 0
        return shard(split_device if splits else per_device)(*args)

    shard = lambda body: jax.shard_map(
        body,
        mesh=mesh,
        in_specs=placed,
        out_specs=P("fs", ("sp", "tp"), None),
        check_vma=False,
    )

    return program
```

profile of v0, /device:TPU:15, one launch (start us, length us, event | category | flops | bytes accessed | tf_op | source)
XLA Modules:
  0.0 278.9 jit_solution(1288530210660851743)
XLA Ops:
  0.0 1.1 copy.16
  1.1 0.1 copy.24
  1.3 1.0 copy.17
  2.3 0.1 copy.25
  2.4 0.0 copy-start.6
  2.5 1.1 copy.18
  3.5 0.1 copy.26
  3.7 0.0 copy-done.4
  3.7 0.2 copy.19
  3.9 0.0 copy-start.8
  3.9 0.1 copy.27
  4.1 0.0 copy-done.5
  4.1 0.0 copy-start.7
  4.1 0.2 copy.20
  4.3 0.1 copy.28
  4.5 0.0 copy-done.6
  4.5 0.2 copy.21
  4.7 0.1 copy.29
  4.9 0.0 copy-done.8
  4.9 0.1 copy.22
  5.0 0.1 copy.30
  5.2 0.2 copy.23
  5.4 0.1 copy.31
  5.5 1.2 copy-done.3
  6.7 105.0 %shard_map.145 = (bf16[4,4,128,1536]{3,2,1,0:T(8,128)(2,1)}, bf16[2,2048,1024]{2,1,0:T(8,128)(2,1)}) custom-call(bf16[4,128,1536]{2,1,0:T(8,128)(2,1)} %bitcast.31, bf16[512,1024]{1,0:T(8,128)(2,1)} %bitcast.33), custom_call_target="tpu_custom_call" | custom-call | tf_op jit(solution)/shard_map/pallas_call | solution.py:309
  111.7 3.9 %slice_bitcast_fusion.1 = (bf16[2048,1024]{1,0:T(8,128)(2,1)S(1)}, bf16[2048,1024]{1,0:T(8,128)(2,1)S(1)}) fusion(bf16[2,2048,1024]{2,1,0:T(8,128)(2,1)} %get-tuple-element.7), kind=kLoop, calls=%fused_computation.12 | loop fusion | bytes 16777216 | tf_op jit(solution)/shard_map/squeeze | solution.py:435
  115.6 0.0 copy-start.9
  115.7 1.9 fusion
  117.6 0.0 copy-done.9
  117.6 13.8 %fusion.3.refs_0_.refs_1_.refs_2_ = f32[2048,1152]{1,0:T(8,128)S(1)} fusion(f32[2048]{0:T(1024)S(1)} %copy-done.9, f32[2048]{0:T(1024)S(1)} %add_rsqrt_fusion, bf16[2048,1024]{1,0:T(8,128)(2,1)S(1)} %get-tuple-element.10, bf16[2048,1024]{1,0:T(8,128)(2,1)S(1)} %get-tuple-element.9, bf16[2048,1536]{1,0:T(8,128)(2,1)} %bitcast.45), kind=kOutput, calls=%fused_computation.5 | convolution fusion | flops 9693036544 | bytes 22560768 | tf_op jit(solution)/shard_map/dot_general | solution.py:437
  131.4 0.2 fusion.8
  131.7 0.2 convert_element_type.28
  131.8 1.1 slice.68
  132.9 3.6 %copy-done = f32[2048,1152]{1,0:T(8,128)} copy-done((f32[2048,1152]{1,0:T(8,128)}, f32[2048,1152]{1,0:T(8,128)S(1)}, u32[]{:S(2)}) %copy-start) | copy-done | bytes 9437208
  136.5 0.9 constant_dynamic-slice_fusion
  137.4 2.1 multiply_convert_fusion
  139.5 0.1 broadcast_in_dim_tile.6.refs_3_
  139.6 0.1 broadcast_in_dim_tile.7.refs_4_
  139.7 0.0 copy-done.12
  139.7 0.6 dynamic_slice.6
  140.2 0.6 broadcast_in_dim.17.refs_5_
  140.9 3.7 %copy-done.1 = f32[2048,1152]{1,0:T(8,128)S(1)} copy-done((f32[2048,1152]{1,0:T(8,128)S(1)}, f32[2048,1152]{1,0:T(8,128)}, u32[]{:S(2)}) %copy-start.1) | copy-done | bytes 9437208
  144.6 18.0 %shard_map.146 = bf16[2048,128]{1,0:T(8,128)(2,1)S(1)} custom-call(f32[2048,1152]{1,0:T(8,128)S(1)} %copy-done.1, f32[2048,1152]{1,0:T(8,128)S(1)} %copy-done.1, f32[2048,1152]{1,0:T(8,128)S(1)} %copy-done.1, f32[1,128]{1,0:T(1,128)S(1)} %broadcast_in_dim_tile.6.refs_3_, f32[1,128]{1,0:T(1,128)S(1)} %broadcast_in_dim_tile.7.refs_4_, ...), custom_call_target="tpu_custom_call" | custom-call | flops 4294967296 | bytes 3670016 | tf_op jit(solution)/shard_map/pallas_call | solution.py:131
  162.6 0.2 pad_maximum_fusion.2
  162.8 0.2 copy.32
  163.0 8.2 %convolution_convert_fusion = bf16[2048,2048]{1,0:T(8,128)(2,1)} fusion(bf16[2048,384]{1,0:T(8,128)(2,1)S(1)} %bitcast.32, bf16[2048,1536]{1,0:T(8,128)(2,1)} %bitcast.46), kind=kOutput, calls=%fused_computation.9 | convolution fusion | flops 3225419776 | bytes 11534336 | tf_op jit(solution)/shard_map/dot_general | solution.py:451
  171.2 106.7 %shard_map.147 = bf16[256,2048]{1,0:T(8,128)(2,1)S(1)} custom-call(bf16[2,4,256,2048]{3,2,1,0:T(8,128)(2,1)} %bitcast.29), custom_call_target="tpu_custom_call" | custom-call | tf_op jit(solution)/shard_map/pallas_call | solution.py:376
  278.0 1.0 copy.41
  (24 shorter events, 0.2 us)
Async XLA Ops:
  0.0 3.7 %copy-start.4 = (bf16[128,1024]{1,0:T(8,128)(2,1)S(1)}, bf16[128,1024]{1,0:T(8,128)(2,1)}, u32[]{:S(2)}) copy-start(bf16[128,1024]{1,0:T(8,128)(2,1)} %param.24) | copy-start | bytes 786436
  0.0 4.1 %copy-start.5 = (bf16[128,1024]{1,0:T(8,128)(2,1)S(1)}, bf16[128,1024]{1,0:T(8,128)(2,1)}, u32[]{:S(2)}) copy-start(bf16[128,1024]{1,0:T(8,128)(2,1)} %param.25) | copy-start | bytes 786436
  2.4 2.1 copy-start.6
  3.9 0.9 copy-start.8
  4.1 1.1 copy-start.7
  5.5 1.2 copy-start.3
  115.6 2.0 copy-start.9
  132.9 3.6 %copy-start = (f32[2048,1152]{1,0:T(8,128)}, f32[2048,1152]{1,0:T(8,128)S(1)}, u32[]{:S(2)}) copy-start(f32[2048,1152]{1,0:T(8,128)S(1)} %fusion.3.refs_0_.refs_1_.refs_2_) | copy-start | bytes 28311556
  137.4 2.1 copy-start.10
  137.4 2.2 copy-start.11
  137.4 2.3 copy-start.12
  137.4 3.5 %copy-start.2 = (f32[128]{0:T(128)S(1)}, f32[128]{0:T(128)}, u32[]{:S(2)}) copy-start(f32[128]{0:T(128)} %param.23) | copy-start | bytes 1540
  140.9 3.7 %copy-start.1 = (f32[2048,1152]{1,0:T(8,128)S(1)}, f32[2048,1152]{1,0:T(8,128)}, u32[]{:S(2)}) copy-start(f32[2048,1152]{1,0:T(8,128)} %copy-done) | copy-start | bytes 28311556
where the time goes:
time: 279 us
  Pallas kernels  230 us (82%)
  local copies, waits for them, and re-layouts  22.2 us (8%)
  matrix products  22 us (8%)
  other arithmetic  4.59 us (2%)
    pallas_call x1, Pallas kernels, reduce_all(): pl.pallas_call(lambda *refs: reduce_kernel(n, *refs), out_shape=jax.Shape...  107 us
    pallas_call x1, Pallas kernels, gather_all(): pl.pallas_call(lambda *refs: gather_kernel(n, *refs), out_shape=(jax.Shap...  105 us
    pallas_call x1, Pallas kernels, attention_call(): pl.pallas_call(lambda *refs: attention_kernel(half, *refs), out_shape=jax...  18 us
    dot_general x1, matrix products, split_device(): y = jnp.dot(normed, into, preferred_element_type=jnp.float32)  13.8 us
    unnamed x42, local copies, waits for them, and re-layouts  13.6 us
    dot_general x1, matrix products, split_device(): lax.dot_general(hidden, outof, (((1,), (1,)), ((), ())), preferred_elemen...  8.23 us

commit v1 on v0

v1 whole, which is shorter than its diff:
```python
import math

import jax
import jax.numpy as jnp
from jax import lax
from jax.experimental import pallas as pl
from jax.experimental.pallas import tpu as pltpu
from jax.sharding import PartitionSpec as P

epsilon = 1e-06


def padded_2(x, sides, width):
    for axis, dim in sides:
        size, length = (lax.axis_size(axis), x.shape[dim])
        up = [(i, (i + 1) % size) for i in range(size - 1)]
        down = [(j, i) for i, j in up]
        last = lax.slice_in_dim(x, length - width, length, axis=dim)
        initial = lax.slice_in_dim(x, 0, width, axis=dim)
        before = lax.ppermute(last, axis, up)
        after = lax.ppermute(initial, axis, down)
        x = jnp.concatenate([before, x, after], axis=dim)
    return x


def scale_rows(values, gain):
    return values * lax.rsqrt(jnp.mean(values * values, axis=-1, keepdims=True) + epsilon) * gain


def project_all(normed, weights, products):
    result = []
    for member in range(len(weights)):
        if member < products:
            result.append(jnp.dot(normed, weights[member], preferred_element_type=jnp.float32))
        else:
            result.append(weights[member])
    return tuple(result)


def attention_branch(query, key, values, weight_two, query_gain, key_gain, head_gain):
    tok_rows = query.shape[0]
    vsize = head_gain.shape[0]
    half = query_gain.shape[0]
    heads = values.shape[1] // vsize
    query_normed = scale_rows(query.reshape(tok_rows, heads, 2, half), query_gain).astype(
        jnp.bfloat16
    )
    key_normed = scale_rows(key.reshape(tok_rows, heads * 2, half), key_gain).astype(jnp.bfloat16)
    key_normed = key_normed.reshape(tok_rows, heads * 2 * half)
    scale = half ** (-0.5)
    initial = (
        jnp.full((heads, 2, tok_rows), -1e30, jnp.float32),
        jnp.zeros((heads, 2, tok_rows), jnp.float32),
        jnp.zeros((heads, 2, tok_rows, vsize), jnp.float32),
    )
    carry = initial
    key_piece = lax.all_gather(key_normed, "sp", axis=0, tiled=True)
    value_piece = lax.all_gather(values, "sp", axis=0, tiled=True)
    length = key_piece.shape[0]
    block = math.gcd(length, 512)
    key_blocks = key_piece.reshape(length // block, block, heads, 2, half)
    value_blocks = value_piece.reshape(length // block, block, heads, vsize)

    def one_block(state, blocks):
        peak, total, accum = state
        key_block, value_block = blocks
        scores = (
            jnp.einsum(
                "qhjd,khjd->hjqk", query_normed, key_block, preferred_element_type=jnp.float32
            )
            * scale
        )
        new_peak = jnp.maximum(peak, jnp.max(scores, axis=-1))
        factor = jnp.exp(peak - new_peak)
        expo = jnp.exp(scores - new_peak[..., None])
        total = total * factor + jnp.sum(expo, axis=-1)
        accum = accum * factor[..., None] + jnp.einsum(
            "hjqk,khd->hjqd",
            expo.astype(jnp.bfloat16),
            value_block,
            preferred_element_type=jnp.float32,
        )
        return ((new_peak, total, accum), None)

    carry, unused = lax.scan(one_block, carry, (key_blocks, value_blocks))
    peak, total, accum = carry
    mapped = accum / total[..., None]
    head_out = mapped[:, 0] - weight_two[:, None, None] * mapped[:, 1]
    normed_out = scale_rows(head_out, head_gain).astype(jnp.bfloat16)
    return jnp.transpose(normed_out, (1, 0, 2)).reshape(tok_rows, heads * vsize)


def half_scaled(values, gain, half):
    low = lax.broadcasted_iota(jnp.int32, (1, 2 * half), 1) < half
    squares = values * values
    first = jnp.sum(jnp.where(low, squares, 0.0), axis=-1, keepdims=True) / half
    second = jnp.sum(jnp.where(low, 0.0, squares), axis=-1, keepdims=True) / half
    factor = jnp.where(low, lax.rsqrt(first + epsilon), lax.rsqrt(second + epsilon))
    return values * factor * gain


def remote(source, target, send, recv, where):
    return pltpu.make_async_remote_copy(
        src_ref=source,
        dst_ref=target,
        send_sem=send,
        recv_sem=recv,
        device_id=where,
        device_id_type=pl.DeviceIdType.MESH,
    )


def meet(places):
    barrier = pltpu.get_barrier_semaphore()
    for where in places:
        pl.semaphore_signal(
            barrier, inc=1, device_id=where, device_id_type=pl.DeviceIdType.MESH
        )
    pl.semaphore_wait(barrier, len(places))


def load(source, target, sem):
    return pltpu.make_async_copy(source, target, sem)


def choose(table, z):
    value = table[0]
    for at in range(1, len(table)):
        value = jnp.where(z == at, table[at], value)
    return value


def fused_kernel(
    n, half, tok_ref, q_ref, k_ref, v_ref, post_ref, pre_ref, inner_ref, ao_ref, co_ref,
    gain_ref, qg_ref, kg_ref, lam_ref, hg_ref, taps_ref, out_ref,
    pack, w_all, t_raw, t_twin, t_all, o_raw, wo_all, query, key, val, post, signal, conv_hid,
    attn_hid, hin, mine, give, take,
    l_sem, z_send, z_recv, f_send, f_recv, g_send, g_recv, r_send, r_recv, t_send, t_recv,
    p_send, p_recv, o_send, o_recv, of_send, of_recv, og_send, og_recv, c_send, c_recv,
    a_send, a_recv, e_send, e_recv,
):
    z, f, c = lax.axis_index("sp"), lax.axis_index("fs"), lax.axis_index("tp")
    beside, above = f + 1 - 2 * (f % 2), f + 2 - 4 * (f // 2)
    near = sorted(range(1, n), key=lambda d: min(d, n - d))
    fs = wo_all.shape[0] // n
    rows = tok_ref.shape[0]
    w_rows = q_ref.shape[0]
    total_rows = rows * n
    vsize = v_ref.shape[1] // n
    channels = post_ref.shape[1] // n
    wide = 2 * half
    o_attn = ao_ref.shape[1]
    bf16, f32 = jnp.bfloat16, jnp.float32

    members = ((q_ref, wide), (k_ref, wide), (pre_ref, channels), (inner_ref, channels),
               (post_ref, channels), (v_ref, vsize))
    starts = [0]
    for ref, width in members:
        starts.append(starts[-1] + width)

    def w_place(s, g):
        return w_all.at[pl.ds(pl.multiple_of((s * fs + g) * w_rows, w_rows), w_rows)]

    tok_load = load(tok_ref, t_raw, l_sem.at[n * 6])
    tok_load.start()
    loads = {}
    for d in near + [0]:
        to = (z + d) % n
        target = pack.at[d] if d else w_place(z, f)
        loads[d] = []
        for m, (ref, width) in enumerate(members):
            piece = load(
                ref.at[:, pl.ds(pl.multiple_of(to * width, width), width)],
                target.at[:, pl.ds(starts[m], width)],
                l_sem.at[d * 6 + m],
            )
            piece.start()
            loads[d].append(piece)
    o_loads = [
        load(ao_ref, o_raw.at[:, pl.ds(0, o_attn)], l_sem.at[n * 6 + 1]),
        load(co_ref, o_raw.at[:, pl.ds(o_attn, co_ref.shape[1])], l_sem.at[n * 6 + 2]),
    ]
    for piece in o_loads:
        piece.start()

    meet([{"sp": (z + d) % n} for d in near] + [{"fs": beside}, {"fs": above}, {"tp": 1 - c}])

    flights = []

    def go(copy):
        copy.start()
        flights.append(copy)
        return copy

    tok_load.wait()
    raw = go(remote(t_raw, t_twin, r_send.at[0], r_recv.at[0], {"tp": 1 - c}))
    across = {}
    for d in near:
        for piece in loads[d]:
            piece.wait()
        across[d] = go(
            remote(pack.at[d], w_place(z, f), z_send.at[d], z_recv.at[d], {"sp": (z + d) % n})
        )
    for piece in loads[0]:
        piece.wait()
    side = {}

    def spread(d):
        s = (z + n - d) % n
        for i, to in enumerate((beside, above)):
            side[i, d] = go(
                remote(w_place(s, f), w_place(s, f), f_send.at[i, d], f_recv.at[i, d], {"fs": to})
            )

    further = {}

    def pass_on(d):
        s = (z + n - d) % n
        i = d % 2
        side[i, d].wait_recv()
        held, to = (beside, above) if i == 0 else (above, beside)
        further[d] = go(
            remote(w_place(s, held), w_place(s, held), g_send.at[d], g_recv.at[d], {"fs": to})
        )

    spread(0)

    raw.wait_recv()
    tile = math.gcd(rows, 64)

    def norm_rows(i, unused):
        at = pl.ds(pl.multiple_of(i * tile, tile), tile)
        to = pl.ds(pl.multiple_of(z * rows + i * tile, tile), tile)
        own, twin = t_raw[at, :].astype(f32), t_twin[at, :].astype(f32)
        square = jnp.sum(own * own, axis=-1, keepdims=True) + jnp.sum(
            twin * twin, axis=-1, keepdims=True
        )
        factor = lax.rsqrt(square / (2 * own.shape[1]) + epsilon)
        t_all[c, to, :] = (own * factor * gain_ref[c]).astype(bf16)
        t_all[1 - c, to, :] = (twin * factor * gain_ref[1 - c]).astype(bf16)
        return unused

    lax.fori_loop(0, rows // tile, norm_rows, 0)

    def t_place(s):
        return t_all.at[c, pl.ds(pl.multiple_of(s * rows, rows), rows)]

    def t_along(s, step):
        return remote(
            t_place(s), t_place(s), t_send.at[(step + 1) // 2, s], t_recv.at[s], {"sp": z + step}
        )

    def t_aside(s):
        return remote(t_place(s), t_place(s), p_send.at[s], p_recv.at[s], {"tp": 1 - c})

    def o_place(s, g):
        return wo_all.at[s * fs + g]

    def o_along(s, step):
        return remote(
            o_place(s, f), o_place(s, f), o_send.at[(step + 1) // 2, s], o_recv.at[s],
            {"sp": z + step},
        )

    def o_side(s, i):
        return remote(
            o_place(s, f), o_place(s, f), of_send.at[i, s], of_recv.at[i, s],
            {"fs": (beside, above)[i]},
        )

    def o_further(s, d):
        held, to = (beside, above) if d % 2 == 0 else (above, beside)
        return remote(
            o_place(s, held), o_place(s, held), og_send.at[s], og_recv.at[s], {"fs": to}
        )

    def both_ways(along):
        for step in (1, -1):
            @pl.when(jnp.logical_and(z + step >= 0, z + step < n))
            def _(step=step):
                along(z, step).start()

    both_ways(t_along)

    for piece in o_loads:
        piece.wait()
    square = o_raw.shape[0]
    for i in range(o_raw.shape[1] // square):
        wo_all[z * fs + f, i * square:(i + 1) * square, :] = o_raw[
            :, i * square:(i + 1) * square
        ].T
    both_ways(o_along)

    last = 0
    for d in near:
        across[d].wait_recv()
        spread(d)
        pass_on(last)
        last = d
    pass_on(last)
    for i in range(2):
        o_side(z, i).start()
    for d in range(n):
        side[1 - d % 2, d].wait_recv()
        further[d].wait_recv()

    order = [sorted(range(n), key=lambda s: (abs(s - at), s > at if 2 * at < n else s < at))
             for at in range(n)]

    def t_event(at, s):
        t_along(s, 1).wait_recv()
        step = 1 if s < at else -1
        if 0 <= at + step < n:
            t_along(s, step).start()
        t_aside(s).start()

    def o_event(at, s):
        o_along(s, 1).wait_recv()
        step = 1 if s < at else -1
        if 0 <= at + step < n:
            o_along(s, step).start()
        for i in range(2):
            o_side(s, i).start()

    def o_pass(at, s):
        d = (at - s) % n
        o_side(s, d % 2).wait_recv()
        o_further(s, d).start()

    plans = []
    for at in range(n):
        plan = [[] for _ in range(n + 1)]
        t_done, o_done, p_done = {at}, {at}, set()
        for visit in range(1, n):
            s = order[at][visit]
            for r in order[at]:
                if abs(r - at) < abs(s - at) and r not in o_done:
                    plan[visit].append((o_event, r))
                    o_done.add(r)
            if s not in t_done:
                for r in order[at]:
                    if abs(r - at) == abs(s - at):
                        plan[visit].append((t_event, r))
                        t_done.add(r)
            elif s not in o_done:
                for r in order[at]:
                    if abs(r - at) == abs(s - at):
                        plan[visit].append((o_event, r))
                        o_done.add(r)
            ready = [r for r in order[at] if r in o_done and r not in p_done]
            if visit == 1 or visit == n - 1:
                for r in ready:
                    plan[visit].append((o_pass, r))
                    p_done.add(r)
        for r in order[at]:
            if r not in o_done:
                plan[n - 1 + 1].append((o_event, r))
        plans.append((plan, [r for r in order[at] if r not in p_done]))

    def follow(stage):
        for at in range(n):
            if plans[at][0][stage]:
                @pl.when(z == at)
                def _(at=at):
                    for event, s in plans[at][0][stage]:
                        event(at, s)

    deep = t_all.shape[2]
    m_rows = math.gcd(rows, 256)

    def project(s):
        def some(i, unused):
            base = pl.multiple_of(s * rows + i * m_rows, m_rows)
            at = pl.ds(base, m_rows)

            def product(first, final):
                lo, hi = starts[first], starts[final]
                return jnp.dot(
                    t_all[0, at, :], w_all[0:deep, lo:hi], preferred_element_type=f32
                ) + jnp.dot(
                    t_all[1, at, :], w_all[deep:2 * deep, lo:hi], preferred_element_type=f32
                )

            pair = product(0, 2)
            low = lax.broadcasted_iota(jnp.int32, (1, wide), 1) < half
            q = half_scaled(pair[:, :wide], qg_ref[...], half).astype(bf16).astype(f32)
            query[0, at, :] = jnp.where(low, q, 0.0).astype(bf16)
            query[1, at, :] = jnp.where(low, 0.0, q).astype(bf16)
            key[at, :] = half_scaled(pair[:, wide:], kg_ref[...], half).astype(bf16)
            mixed = product(2, 3) * product(3, 4)
            signal[pl.ds(base + 8, m_rows), :] = mixed.astype(bf16).astype(f32)
            post[at, :] = product(4, 5).astype(bf16)
            val[at, :] = product(5, 6).astype(bf16)
            return unused

        lax.fori_loop(0, rows // m_rows, some, 0)

    signal[0:8, :] = jnp.zeros((8, channels), f32)
    signal[total_rows + 8:total_rows + 16, :] = jnp.zeros((8, channels), f32)
    project(z)
    for visit in range(1, n):
        follow(visit)
        s = choose([order[at][visit] for at in range(n)], z)
        t_aside(s).wait_recv()
        project(s)

    place = c * n + z
    taps = taps_ref[:, pl.ds(pl.multiple_of(place * channels, channels), channels)]
    h_rows = math.gcd(rows, 64)

    def convolve(i, unused):
        base = pl.multiple_of(i * h_rows, h_rows)
        around = signal[pl.ds(base, h_rows + 16), :]
        before = around[7:7 + h_rows]
        middle = around[8:8 + h_rows]
        after = around[9:9 + h_rows]
        filtered = taps[0:1] * before + taps[1:2] * middle + taps[2:3] * after
        at = pl.ds(base, h_rows)
        conv_hid[at, :] = (post[at, :].astype(f32) * filtered).astype(bf16)
        return unused

    lax.fori_loop(0, total_rows // h_rows, convolve, 0)
    conv_at = pl.ds(pl.multiple_of(o_attn + z * channels, channels), channels)
    attn_at = pl.ds(pl.multiple_of(z * vsize, vsize), vsize)

    def c_copy(d):
        to = (z + d) % n
        return remote(
            conv_hid.at[pl.ds(pl.multiple_of(to * rows, rows), rows)], hin.at[:, conv_at],
            c_send.at[d], c_recv.at[d], {"sp": to},
        )

    def a_copy(d):
        to = (z + d) % n
        return remote(
            attn_hid.at[pl.ds(pl.multiple_of(to * rows, rows), rows)], hin.at[:, attn_at],
            a_send.at[d], a_recv.at[d], {"sp": to},
        )

    far = near[::-1]
    for d in far:
        c_copy(d).start()
    own = pl.ds(pl.multiple_of(z * rows, rows), rows)
    hin[:, conv_at] = conv_hid[own, :]

    a_rows = math.gcd(rows, 256)
    each = rows // a_rows
    scale = half ** (-0.5) * math.log2(math.e)
    lam = lam_ref[place]

    def attend(i, unused):
        @pl.when(i == 2)
        def _():
            follow(n)

        d = choose(far + [0], i // each)
        at = pl.ds(pl.multiple_of(((z + d) % n) * rows + (i % each) * a_rows, a_rows), a_rows)
        maps = []
        for which in range(2):
            scores = lax.dot_general(
                query[which, at, :], key[...], (((1,), (1,)), ((), ())),
                preferred_element_type=f32,
            ) * scale
            expo = jnp.exp2(scores - jnp.max(scores, axis=-1, keepdims=True))
            total = jnp.sum(expo, axis=-1, keepdims=True)
            maps.append(
                jnp.dot(expo.astype(bf16), val[...], preferred_element_type=f32) / total
            )
        head_out = maps[0] - lam * maps[1]
        attn_hid[at, :] = scale_rows(head_out, hg_ref[...]).astype(bf16)
        for j, d in enumerate(far):
            @pl.when(i == (j + 1) * each - 1)
            def _(d=d):
                a_copy(d).start()
        return unused

    lax.fori_loop(0, n * each, attend, 0)
    hin[:, attn_at] = attn_hid[own, :]
    for at in range(n):
        @pl.when(z == at)
        def _(at=at):
            for s in plans[at][1]:
                o_pass(at, s)

    for s in range(n):
        for i in range(2):
            @pl.when((z + n - s) % 2 != i)
            def _(s=s, i=i):
                o_side(s, i).wait_recv()
        o_further(s, 0).wait_recv()
    for d in far:
        c_copy(d).wait_recv()
        a_copy(d).wait_recv()

    pairs = wo_all.shape[0] // 2
    half_rows = rows // 2

    def swap(j):
        return remote(give.at[j], take.at[j], e_send.at[j], e_recv.at[j], {"tp": 1 - c})

    def produce(j, unused):
        weights = jnp.concatenate([wo_all[2 * j], wo_all[2 * j + 1]], axis=1)
        theirs = pl.ds(pl.multiple_of((1 - c) * half_rows, half_rows), half_rows)
        ours = pl.ds(pl.multiple_of(c * half_rows, half_rows), half_rows)
        give[j] = jnp.dot(hin[theirs, :], weights, preferred_element_type=f32).astype(bf16)
        swap(j).start()
        mine[j] = jnp.dot(hin[ours, :], weights, preferred_element_type=f32).astype(bf16)
        return unused

    lax.fori_loop(0, pairs, produce, 0)
    width = give.shape[2]

    for j in range(pairs):
        swap(j).wait_recv()
        out_ref[:, j * width:(j + 1) * width] = (
            mine[j].astype(f32) + take[j].astype(f32)
        ).astype(bf16)

    for copy in flights:
        copy.wait_send()
    for d in far:
        c_copy(d).wait_send()
        a_copy(d).wait_send()
    for j in range(pairs):
        swap(j).wait_send()
    for s in range(n):
        for i in range(2):
            o_side(s, i).wait_send()
        o_further(s, 0).wait_send()
        for step in (1, -1):
            arrives = s <= z if step == 1 else s >= z
            @pl.when(jnp.logical_and(arrives, jnp.logical_and(z + step >= 0, z + step < n)))
            def _(s=s, step=step):
                t_along(s, step).wait_send()
                o_along(s, step).wait_send()

        @pl.when(z != s)
        def _(s=s):
            t_aside(s).wait_send()


def split_device(
    inputs,
    norm_gain,
    query_weight,
    key_weight,
    value_weight,
    query_gain,
    key_gain,
    mix_lambda,
    head_gain,
    post_gate_weight,
    pre_gate_weight,
    inner_weight,
    conv_taps,
    attn_out_weight,
    conv_out_weight,
):
    n, fs, tp = lax.axis_size("sp"), lax.axis_size("fs"), lax.axis_size("tp")
    tokens = inputs[0]
    rows, deep = tokens.shape
    half, vsize = query_gain.shape[0], head_gain.shape[0]
    channels = post_gate_weight.shape[1] // n
    w_rows = query_weight.shape[0]
    columns = 4 * half + vsize + 3 * channels
    hidden = n * (vsize + channels)
    total = n * rows
    out_width = w_rows * n * fs
    pairs = n * fs // 2
    bf16, dma = jnp.bfloat16, pltpu.SemaphoreType.DMA
    far, close = pl.BlockSpec(memory_space=pl.ANY), pl.BlockSpec(memory_space=pltpu.VMEM)
    result = pl.pallas_call(
        lambda *refs: fused_kernel(n, half, *refs),
        out_shape=jax.ShapeDtypeStruct((rows // tp, out_width), bf16),
        in_specs=[far] * 9 + [close] * 3 + [pl.BlockSpec(memory_space=pltpu.SMEM)] + [close] * 2,
        out_specs=close,
        scratch_shapes=[
            pltpu.VMEM((n, w_rows, columns), bf16),
            pltpu.VMEM((n * fs * w_rows, columns), bf16),
            pltpu.VMEM((rows, deep), bf16),
            pltpu.VMEM((rows, deep), bf16),
            pltpu.VMEM((tp, total, deep), bf16),
            pltpu.VMEM((w_rows, hidden), bf16),
            pltpu.VMEM((n * fs, hidden, w_rows), bf16),
            pltpu.VMEM((2, total, 2 * half), bf16),
            pltpu.VMEM((total, 2 * half), bf16),
            pltpu.VMEM((total, vsize), bf16),
            pltpu.VMEM((total, channels), bf16),
            pltpu.VMEM((total + 16, channels), jnp.float32),
            pltpu.VMEM((total, channels), bf16),
            pltpu.VMEM((total, vsize), bf16),
            pltpu.VMEM((rows, hidden), bf16),
            pltpu.VMEM((pairs, rows // tp, 2 * w_rows), bf16),
            pltpu.VMEM((pairs, rows // tp, 2 * w_rows), bf16),
            pltpu.VMEM((pairs, rows // tp, 2 * w_rows), bf16),
            dma((n * 6 + 3,)),
            dma((n,)), dma((n,)), dma((2, n)), dma((2, n)), dma((n,)), dma((n,)),
            dma((1,)), dma((1,)), dma((2, n)), dma((n,)), dma((n,)), dma((n,)),
            dma((2, n)), dma((n,)), dma((2, n)), dma((2, n)), dma((n,)), dma((n,)),
            dma((n,)), dma((n,)), dma((n,)), dma((n,)), dma((pairs,)), dma((pairs,)),
        ],
        compiler_params=pltpu.CompilerParams(
            collective_id=1, has_side_effects=True, vmem_limit_bytes=60 * 2**20
        ),
    )(
        tokens, query_weight, key_weight, value_weight, post_gate_weight, pre_gate_weight,
        inner_weight, attn_out_weight, conv_out_weight,
        norm_gain.reshape(tp, 1, deep),
        jnp.tile(query_gain, 2)[None],
        jnp.tile(key_gain, 2)[None],
        mix_lambda,
        head_gain[None],
        conv_taps,
    )
    return result[None]


def per_device(
    inputs,
    norm_gain,
    query_weight,
    key_weight,
    value_weight,
    query_gain,
    key_gain,
    mix_lambda,
    head_gain,
    post_gate_weight,
    pre_gate_weight,
    inner_weight,
    conv_taps,
    attn_out_weight,
    conv_out_weight,
):
    tokens = inputs[0]
    whole = lax.all_gather(tokens, "tp", axis=1, tiled=True)
    normed = scale_rows(whole.astype(jnp.float32), norm_gain).astype(jnp.bfloat16)
    heads_dev = value_weight.shape[1] // head_gain.shape[0]
    channels = post_gate_weight.shape[1]
    tp_index = lax.axis_index("tp")
    weight_two = lax.dynamic_slice_in_dim(mix_lambda, tp_index * heads_dev, heads_dev)
    taps = lax.dynamic_slice_in_dim(conv_taps, tp_index * channels, channels, 1)
    every_full = (
        lax.all_gather(query_weight, ("sp", "fs"), axis=0, tiled=True),
        lax.all_gather(key_weight, ("sp", "fs"), axis=0, tiled=True),
        lax.all_gather(value_weight, ("sp", "fs"), axis=0, tiled=True),
        lax.all_gather(post_gate_weight, ("sp", "fs"), axis=0, tiled=True),
        lax.all_gather(pre_gate_weight, ("sp", "fs"), axis=0, tiled=True),
        lax.all_gather(inner_weight, ("sp", "fs"), axis=0, tiled=True),
        lax.all_gather(attn_out_weight, ("sp", "fs"), axis=0, tiled=True),
        lax.all_gather(conv_out_weight, ("sp", "fs"), axis=0, tiled=True),
    )
    query, key, value_proj, post, pre_gate, inner, attn_out_full, conv_out_full = project_all(
        normed, every_full[0:3] + every_full[3:6] + every_full[6:8], 6
    )
    attn_hidden = attention_branch(
        query, key, value_proj.astype(jnp.bfloat16), weight_two, query_gain, key_gain, head_gain
    )
    post_mid = post.astype(jnp.bfloat16)
    post_wide = lax.optimization_barrier(post_mid).astype(jnp.float32)
    signal = (pre_gate * inner).astype(jnp.bfloat16)
    padded = padded_2(signal, (("sp", 0),), 1)
    shifted = lax.optimization_barrier(padded).astype(jnp.float32)
    filtered = taps[0] * shifted[:-2] + taps[1] * shifted[1:-1] + taps[2] * shifted[2:]
    conv_hidden = (post_wide * filtered).astype(jnp.bfloat16)
    contract = (((1,), (1,)), ((), ()))
    summed = lax.psum_scatter(
        (
            lax.dot_general(
                attn_hidden, attn_out_full, contract, preferred_element_type=jnp.float32
            )
            + lax.dot_general(
                conv_hidden, conv_out_full, contract, preferred_element_type=jnp.float32
            )
        ).astype(jnp.bfloat16),
        "tp",
        scatter_dimension=0,
        tiled=True,
    )
    return summed[None]


def solution(mesh):
    placed = (
        P("fs", "sp", "tp"),
        P(),
        P(("sp", "fs"), "tp"),
        P(("sp", "fs"), "tp"),
        P(("sp", "fs"), "tp"),
        P(),
        P(),
        P(),
        P(),
        P(("sp", "fs"), "tp"),
        P(("sp", "fs"), "tp"),
        P(("sp", "fs"), "tp"),
        P(),
        P(("sp", "fs"), "tp"),
        P(("sp", "fs"), "tp"),
    )
    sp, tp = mesh.shape["sp"], mesh.shape["tp"]

    def program(*args):
        heads = args[7].shape[0]
        channels = args[12].shape[1]
        splits = tp == 2 and mesh.shape["fs"] == 4 and sp > 1 and heads == sp * tp
        splits = splits and channels % (sp * tp * 128) == 0
        return shard(split_device if splits else per_device)(*args)

    shard = lambda body: jax.shard_map(
        body,
        mesh=mesh,
        in_specs=placed,
        out_specs=P("fs", ("sp", "tp"), None),
        check_vma=False,
    )

    return program
```

time: 279 us -> 171 us (0.61)
  the two profiles are of different devices: /device:TPU:15 before, /device:TPU:0 now
where the time goes in v1:
time: 171 us; the launch traced here: 170 us
  Pallas kernels  166 us (97%)
  local copies, waits for them, and re-layouts  4.24 us (2%)
    pallas_call x1, Pallas kernels, split_device(): pl.pallas_call(lambda *refs: fused_kernel(n, half, *refs), out_shape=jax....  166 us

profile of v1, /device:TPU:0, one launch (start us, length us, event | category | flops | bytes accessed | tf_op | source)
XLA Modules:
  0.0 170.2 jit_solution(2444092711267376803)
XLA Ops:
  0.0 0.0 copy-start
  0.0 0.7 copy-done
  0.7 0.0 copy-start.1
  0.7 0.6 broadcast_in_dim_tile.6.refs_10_
  1.3 0.1 copy-done.1
  1.3 0.6 broadcast_in_dim_tile.7.refs_11_
  1.9 166.0 %shard_map.145 = bf16[256,2048]{1,0:T(8,128)(2,1)} custom-call(bf16[512,1024]{1,0:T(8,128)(2,1)} %bitcast.5, bf16[128,512]{1,0:T(8,128)(2,1)} %refs_1_.1, bf16[128,512]{1,0:T(8,128)(2,1)} %refs_2_.1, bf16[128,512]{1,0:T(8,128)(2,1)} %refs_3_.1, bf16[128,1024]{1,0:T(8,128)(2,1)} %refs_4_.1, bf16[128,1024]{1,0:T(8,128)(2,1)} %refs_5_.1, ...), custom_call_target="tpu_custom_call" | custom-call | tf_op jit(solution)/shard_map/pallas_call | solution.py:572
  167.9 2.3 %copy.17 = bf16[1,256,2048]{2,1,0:T(8,128)(2,1)} copy(bf16[1,256,2048]{2,1,0:T(8,128)(2,1)} %bitcast.4) | data formatting | bytes 2097152
  (2 shorter events, 0.0 us)
Async XLA Ops:
  0.0 0.7 copy-start
  0.7 0.7 copy-start.1

commit v2 on v1

--- a/solution.py
+++ b/solution.py
@@ -132,17 +132,17 @@
 
 def fused_kernel(
     n, half, tok_ref, q_ref, k_ref, v_ref, post_ref, pre_ref, inner_ref, ao_ref, co_ref,
-    gain_ref, qg_ref, kg_ref, lam_ref, hg_ref, taps_ref, out_ref,
-    pack, w_all, t_raw, t_twin, t_all, o_raw, wo_all, query, key, val, post, signal, conv_hid,
-    attn_hid, hin, mine, give, take,
+    ng_any, qg_any, kg_any, lam_ref, hg_any, taps_any, mine, take,
+    gain_ref, qg_ref, kg_ref, hg_ref, taps_ref, acc, pack, w_all, t_raw, t_twin, t_all, o_raw, wo_all, query, key, val, post, signal, conv_hid,
+    attn_hid, hin, both,
     l_sem, z_send, z_recv, f_send, f_recv, g_send, g_recv, r_send, r_recv, t_send, t_recv,
     p_send, p_recv, o_send, o_recv, of_send, of_recv, og_send, og_recv, c_send, c_recv,
-    a_send, a_recv, e_send, e_recv,
+    a_send, a_recv, e_send, e_recv, s_sem,
 ):
     z, f, c = lax.axis_index("sp"), lax.axis_index("fs"), lax.axis_index("tp")
     beside, above = f + 1 - 2 * (f % 2), f + 2 - 4 * (f // 2)
     near = sorted(range(1, n), key=lambda d: min(d, n - d))
-    fs = wo_all.shape[0] // n
+    fs = 2 * wo_all.shape[0] // n
     rows = tok_ref.shape[0]
     w_rows = q_ref.shape[0]
     total_rows = rows * n
@@ -180,7 +180,15 @@
         load(ao_ref, o_raw.at[:, pl.ds(0, o_attn)], l_sem.at[n * 6 + 1]),
         load(co_ref, o_raw.at[:, pl.ds(o_attn, co_ref.shape[1])], l_sem.at[n * 6 + 2]),
     ]
-    for piece in o_loads:
+    place = c * n + z
+    small = [
+        load(source, target, l_sem.at[n * 6 + 3 + at])
+        for at, (source, target) in enumerate((
+            (ng_any, gain_ref), (qg_any, qg_ref), (kg_any, kg_ref), (hg_any, hg_ref),
+            (taps_any.at[:, pl.ds(pl.multiple_of(place * channels, channels), channels)], taps_ref),
+        ))
+    ]
+    for piece in o_loads + small:
         piece.start()
 
     meet([{"sp": (z + d) % n} for d in near] + [{"fs": beside}, {"fs": above}, {"tp": 1 - c}])
@@ -225,6 +233,8 @@
 
     spread(0)
 
+    for piece in small:
+        piece.wait()
     raw.wait_recv()
     tile = math.gcd(rows, 64)
 
@@ -254,7 +264,8 @@
         return remote(t_place(s), t_place(s), p_send.at[s], p_recv.at[s], {"tp": 1 - c})
 
     def o_place(s, g):
-        return wo_all.at[s * fs + g]
+        at = s * fs + g
+        return wo_all.at[at // 2, :, pl.ds(pl.multiple_of(at % 2 * w_rows, w_rows), w_rows)]
 
     def o_along(s, step):
         return remote(
@@ -286,9 +297,10 @@
         piece.wait()
     square = o_raw.shape[0]
     for i in range(o_raw.shape[1] // square):
-        wo_all[z * fs + f, i * square:(i + 1) * square, :] = o_raw[
-            :, i * square:(i + 1) * square
-        ].T
+        wo_all[
+            (z * fs + f) // 2, i * square:(i + 1) * square,
+            pl.ds(pl.multiple_of(f % 2 * w_rows, w_rows), w_rows),
+        ] = o_raw[:, i * square:(i + 1) * square].T
     both_ways(o_along)
 
     last = 0
@@ -329,44 +341,36 @@
 
     plans = []
     for at in range(n):
-        plan = [[] for _ in range(n + 1)]
-        t_done, o_done, p_done = {at}, {at}, set()
+        plan, t_done, o_done, passed = [], {at}, [at], []
         for visit in range(1, n):
+            events, held = [], [r for r in o_done if r not in passed]
             s = order[at][visit]
-            for r in order[at]:
-                if abs(r - at) < abs(s - at) and r not in o_done:
-                    plan[visit].append((o_event, r))
-                    o_done.add(r)
             if s not in t_done:
-                for r in order[at]:
-                    if abs(r - at) == abs(s - at):
-                        plan[visit].append((t_event, r))
-                        t_done.add(r)
-            elif s not in o_done:
-                for r in order[at]:
-                    if abs(r - at) == abs(s - at):
-                        plan[visit].append((o_event, r))
-                        o_done.add(r)
-            ready = [r for r in order[at] if r in o_done and r not in p_done]
-            if visit == 1 or visit == n - 1:
-                for r in ready:
-                    plan[visit].append((o_pass, r))
-                    p_done.add(r)
-        for r in order[at]:
-            if r not in o_done:
-                plan[n - 1 + 1].append((o_event, r))
-        plans.append((plan, [r for r in order[at] if r not in p_done]))
-
-    def follow(stage):
+                ring = [r for r in order[at] if abs(r - at) == abs(s - at)]
+                events += [(t_event, r) for r in ring]
+                t_done |= set(ring)
+                if visit + len(ring) < n:
+                    events += [(o_event, r) for r in ring]
+                    o_done += ring
+            plan.append(events + [(o_pass, r) for r in held])
+            passed += held
+        plan.append([(o_event, r) for r in order[at] if r not in o_done])
+        plan.append([(o_pass, r) for r in order[at] if r not in passed])
+        plans.append(plan)
+
+    def follow(events):
         for at in range(n):
-            if plans[at][0][stage]:
+            if events(at):
                 @pl.when(z == at)
                 def _(at=at):
-                    for event, s in plans[at][0][stage]:
+                    for event, s in events(at):
                         event(at, s)
 
     deep = t_all.shape[2]
     m_rows = math.gcd(rows, 256)
+
+    q_gain = jnp.concatenate([qg_ref[...], qg_ref[...]], axis=1)
+    k_gain = jnp.concatenate([kg_ref[...], kg_ref[...]], axis=1)
 
     def project(s):
         def some(i, unused):
@@ -383,10 +387,10 @@
 
             pair = product(0, 2)
             low = lax.broadcasted_iota(jnp.int32, (1, wide), 1) < half
-            q = half_scaled(pair[:, :wide], qg_ref[...], half).astype(bf16).astype(f32)
+            q = half_scaled(pair[:, :wide], q_gain, half).astype(bf16).astype(f32)
             query[0, at, :] = jnp.where(low, q, 0.0).astype(bf16)
             query[1, at, :] = jnp.where(low, 0.0, q).astype(bf16)
-            key[at, :] = half_scaled(pair[:, wide:], kg_ref[...], half).astype(bf16)
+            key[at, :] = half_scaled(pair[:, wide:], k_gain, half).astype(bf16)
             mixed = product(2, 3) * product(3, 4)
             signal[pl.ds(base + 8, m_rows), :] = mixed.astype(bf16).astype(f32)
             post[at, :] = product(4, 5).astype(bf16)
@@ -397,51 +401,76 @@
 
     signal[0:8, :] = jnp.zeros((8, channels), f32)
     signal[total_rows + 8:total_rows + 16, :] = jnp.zeros((8, channels), f32)
+    h_rows = math.gcd(rows, 64)
+    conv_at = pl.ds(pl.multiple_of(o_attn + z * channels, channels), channels)
+    attn_at = pl.ds(pl.multiple_of(z * vsize, vsize), vsize)
+    own = pl.ds(pl.multiple_of(z * rows, rows), rows)
+
+    def convolve(s):
+        def some(i, unused):
+            base = pl.multiple_of(s * rows + i * h_rows, h_rows)
+            around = signal[pl.ds(base, h_rows + 16), :]
+            filtered = (
+                taps_ref[0:1] * around[7:7 + h_rows]
+                + taps_ref[1:2] * around[8:8 + h_rows]
+                + taps_ref[2:3] * around[9:9 + h_rows]
+            )
+            at = pl.ds(base, h_rows)
+            conv_hid[at, :] = (post[at, :].astype(f32) * filtered).astype(bf16)
+            return unused
+
+        lax.fori_loop(0, rows // h_rows, some, 0)
+
+    def sent_to(source, columns, to, send, recv):
+        return remote(
+            source.at[pl.ds(pl.multiple_of(to * rows, rows), rows)], hin.at[:, columns],
+            send.at[to], recv.at[z], {"sp": to},
+        )
+
+    def c_copy(to):
+        return sent_to(conv_hid, conv_at, to, c_send, c_recv)
+
+    def a_copy(to):
+        return sent_to(attn_hid, attn_at, to, a_send, a_recv)
+
+    def convolve_send(s):
+        @pl.when(s != z)
+        def _():
+            c_copy(s).start()
+
+    whole = []
+    for at in range(n):
+        seen, out, stages = {at}, set(), []
+        for visit in range(1, n):
+            seen.add(order[at][visit])
+            fresh = [r for r in order[at] if r not in out
+                     and all(q in seen for q in (r - 1, r, r + 1) if 0 <= q < n)]
+            out |= set(fresh)
+            stages.append(fresh)
+        whole.append(stages)
+    counts = [max(len(whole[at][v]) for at in range(n)) for v in range(n - 1)]
+
+    def each_whole(visit, act):
+        for k in range(counts[visit - 1]):
+            held = [whole[at][visit - 1] for at in range(n)]
+            s = choose([p[k] if k < len(p) else -1 for p in held], z)
+            if all(k < len(p) for p in held):
+                act(s)
+            else:
+                @pl.when(s >= 0)
+                def _(s=s):
+                    act(s)
+
     project(z)
     for visit in range(1, n):
-        follow(visit)
+        follow(lambda at: plans[at][visit - 1])
         s = choose([order[at][visit] for at in range(n)], z)
         t_aside(s).wait_recv()
         project(s)
-
-    place = c * n + z
-    taps = taps_ref[:, pl.ds(pl.multiple_of(place * channels, channels), channels)]
-    h_rows = math.gcd(rows, 64)
-
-    def convolve(i, unused):
-        base = pl.multiple_of(i * h_rows, h_rows)
-        around = signal[pl.ds(base, h_rows + 16), :]
-        before = around[7:7 + h_rows]
-        middle = around[8:8 + h_rows]
-        after = around[9:9 + h_rows]
-        filtered = taps[0:1] * before + taps[1:2] * middle + taps[2:3] * after
-        at = pl.ds(base, h_rows)
-        conv_hid[at, :] = (post[at, :].astype(f32) * filtered).astype(bf16)
-        return unused
-
-    lax.fori_loop(0, total_rows // h_rows, convolve, 0)
-    conv_at = pl.ds(pl.multiple_of(o_attn + z * channels, channels), channels)
-    attn_at = pl.ds(pl.multiple_of(z * vsize, vsize), vsize)
-
-    def c_copy(d):
-        to = (z + d) % n
-        return remote(
-            conv_hid.at[pl.ds(pl.multiple_of(to * rows, rows), rows)], hin.at[:, conv_at],
-            c_send.at[d], c_recv.at[d], {"sp": to},
-        )
-
-    def a_copy(d):
-        to = (z + d) % n
-        return remote(
-            attn_hid.at[pl.ds(pl.multiple_of(to * rows, rows), rows)], hin.at[:, attn_at],
-            a_send.at[d], a_recv.at[d], {"sp": to},
-        )
-
+        each_whole(visit, convolve)
+        each_whole(visit, convolve_send)
+    hin[:, conv_at] = conv_hid[own, :]
     far = near[::-1]
-    for d in far:
-        c_copy(d).start()
-    own = pl.ds(pl.multiple_of(z * rows, rows), rows)
-    hin[:, conv_at] = conv_hid[own, :]
 
     a_rows = math.gcd(rows, 256)
     each = rows // a_rows
@@ -449,9 +478,10 @@
     lam = lam_ref[place]
 
     def attend(i, unused):
-        @pl.when(i == 2)
-        def _():
-            follow(n)
+        for k, when in enumerate((0, (n * each) // 2 + 1)):
+            @pl.when(i == when)
+            def _(k=k):
+                follow(lambda at: plans[at][n - 1 + k])
 
         d = choose(far + [0], i // each)
         at = pl.ds(pl.multiple_of(((z + d) % n) * rows + (i % each) * a_rows, a_rows), a_rows)
@@ -471,56 +501,72 @@
         for j, d in enumerate(far):
             @pl.when(i == (j + 1) * each - 1)
             def _(d=d):
-                a_copy(d).start()
+                a_copy((z + d) % n).start()
         return unused
 
     lax.fori_loop(0, n * each, attend, 0)
     hin[:, attn_at] = attn_hid[own, :]
-    for at in range(n):
-        @pl.when(z == at)
-        def _(at=at):
-            for s in plans[at][1]:
-                o_pass(at, s)
-
-    for s in range(n):
+
+    def arrived(source, columns, d, send, recv):
+        s = (z + d) % n
+        remote(
+            source.at[pl.ds(0, rows)], hin.at[:, columns], send.at[s], recv.at[s], {"sp": s}
+        ).wait_recv()
+
+    for d in near:
+        arrived(conv_hid, conv_at, d, c_send, c_recv)
+
+    pairs = wo_all.shape[0]
+    half_rows = rows // 2
+    width = 2 * w_rows
+
+    theirs = pl.ds(pl.multiple_of((1 - c) * half_rows, half_rows), half_rows)
+    ours = pl.ds(pl.multiple_of(c * half_rows, half_rows), half_rows)
+
+    def swap(j):
+        at = pl.ds(pl.multiple_of(j * width, width), width)
+        return remote(
+            both.at[j, theirs], take.at[:, at], e_send.at[j], e_recv.at[j], {"tp": 1 - c}
+        )
+
+    def store(j):
+        at = pl.ds(pl.multiple_of(j * width, width), width)
+        return load(both.at[j, ours], mine.at[:, at], s_sem.at[j])
+
+    def channel_part(j, unused):
+        acc[j] = jnp.dot(hin[:, o_attn:], wo_all[j, o_attn:, :], preferred_element_type=f32)
+        return unused
+
+    for visit in range(n):
+        s = choose([order[at][visit] for at in range(n)], z)
         for i in range(2):
             @pl.when((z + n - s) % 2 != i)
             def _(s=s, i=i):
                 o_side(s, i).wait_recv()
         o_further(s, 0).wait_recv()
-    for d in far:
-        c_copy(d).wait_recv()
-        a_copy(d).wait_recv()
-
-    pairs = wo_all.shape[0] // 2
-    half_rows = rows // 2
-
-    def swap(j):
-        return remote(give.at[j], take.at[j], e_send.at[j], e_recv.at[j], {"tp": 1 - c})
-
-    def produce(j, unused):
-        weights = jnp.concatenate([wo_all[2 * j], wo_all[2 * j + 1]], axis=1)
-        theirs = pl.ds(pl.multiple_of((1 - c) * half_rows, half_rows), half_rows)
-        ours = pl.ds(pl.multiple_of(c * half_rows, half_rows), half_rows)
-        give[j] = jnp.dot(hin[theirs, :], weights, preferred_element_type=f32).astype(bf16)
+        lax.fori_loop(s * (fs // 2), (s + 1) * (fs // 2), channel_part, 0)
+    for d in near:
+        arrived(attn_hid, attn_at, d, a_send, a_recv)
+
+    def head_part(j, unused):
+        both[j] = (
+            acc[j]
+            + jnp.dot(hin[:, :o_attn], wo_all[j, :o_attn, :], preferred_element_type=f32)
+        ).astype(bf16)
         swap(j).start()
-        mine[j] = jnp.dot(hin[ours, :], weights, preferred_element_type=f32).astype(bf16)
+        store(j).start()
         return unused
 
-    lax.fori_loop(0, pairs, produce, 0)
-    width = give.shape[2]
-
+    lax.fori_loop(0, pairs, head_part, 0)
     for j in range(pairs):
         swap(j).wait_recv()
-        out_ref[:, j * width:(j + 1) * width] = (
-            mine[j].astype(f32) + take[j].astype(f32)
-        ).astype(bf16)
+        store(j).wait()
 
     for copy in flights:
         copy.wait_send()
     for d in far:
-        c_copy(d).wait_send()
-        a_copy(d).wait_send()
+        c_copy((z + d) % n).wait_send()
+        a_copy((z + d) % n).wait_send()
     for j in range(pairs):
         swap(j).wait_send()
     for s in range(n):
@@ -568,20 +614,26 @@
     out_width = w_rows * n * fs
     pairs = n * fs // 2
     bf16, dma = jnp.bfloat16, pltpu.SemaphoreType.DMA
-    far, close = pl.BlockSpec(memory_space=pl.ANY), pl.BlockSpec(memory_space=pltpu.VMEM)
-    result = pl.pallas_call(
+    far = pl.BlockSpec(memory_space=pl.ANY)
+    mine, take = pl.pallas_call(
         lambda *refs: fused_kernel(n, half, *refs),
-        out_shape=jax.ShapeDtypeStruct((rows // tp, out_width), bf16),
-        in_specs=[far] * 9 + [close] * 3 + [pl.BlockSpec(memory_space=pltpu.SMEM)] + [close] * 2,
-        out_specs=close,
+        out_shape=(jax.ShapeDtypeStruct((rows // tp, out_width), bf16),) * 2,
+        in_specs=[far] * 12 + [pl.BlockSpec(memory_space=pltpu.SMEM)] + [far] * 2,
+        out_specs=(far, far),
         scratch_shapes=[
+            pltpu.VMEM((tp, 1, deep), jnp.float32),
+            pltpu.VMEM((1, half), jnp.float32),
+            pltpu.VMEM((1, half), jnp.float32),
+            pltpu.VMEM((1, vsize), jnp.float32),
+            pltpu.VMEM((3, channels), jnp.float32),
+            pltpu.VMEM((pairs, rows, 2 * w_rows), jnp.float32),
             pltpu.VMEM((n, w_rows, columns), bf16),
             pltpu.VMEM((n * fs * w_rows, columns), bf16),
             pltpu.VMEM((rows, deep), bf16),
             pltpu.VMEM((rows, deep), bf16),
             pltpu.VMEM((tp, total, deep), bf16),
             pltpu.VMEM((w_rows, hidden), bf16),
-            pltpu.VMEM((n * fs, hidden, w_rows), bf16),
+            pltpu.VMEM((pairs, hidden, 2 * w_rows), bf16),
             pltpu.VMEM((2, total, 2 * half), bf16),
             pltpu.VMEM((total, 2 * half), bf16),
             pltpu.VMEM((total, vsize), bf16),
@@ -590,14 +642,12 @@
             pltpu.VMEM((total, channels), bf16),
             pltpu.VMEM((total, vsize), bf16),
             pltpu.VMEM((rows, hidden), bf16),
-            pltpu.VMEM((pairs, rows // tp, 2 * w_rows), bf16),
-            pltpu.VMEM((pairs, rows // tp, 2 * w_rows), bf16),
-            pltpu.VMEM((pairs, rows // tp, 2 * w_rows), bf16),
-            dma((n * 6 + 3,)),
+            pltpu.VMEM((pairs, rows, 2 * w_rows), bf16),
+            dma((n * 6 + 8,)),
             dma((n,)), dma((n,)), dma((2, n)), dma((2, n)), dma((n,)), dma((n,)),
             dma((1,)), dma((1,)), dma((2, n)), dma((n,)), dma((n,)), dma((n,)),
             dma((2, n)), dma((n,)), dma((2, n)), dma((2, n)), dma((n,)), dma((n,)),
-            dma((n,)), dma((n,)), dma((n,)), dma((n,)), dma((pairs,)), dma((pairs,)),
+            dma((n,)), dma((n,)), dma((n,)), dma((n,)), dma((pairs,)), dma((pairs,)), dma((pairs,)),
         ],
         compiler_params=pltpu.CompilerParams(
             collective_id=1, has_side_effects=True, vmem_limit_bytes=60 * 2**20
@@ -606,13 +656,13 @@
         tokens, query_weight, key_weight, value_weight, post_gate_weight, pre_gate_weight,
         inner_weight, attn_out_weight, conv_out_weight,
         norm_gain.reshape(tp, 1, deep),
-        jnp.tile(query_gain, 2)[None],
-        jnp.tile(key_gain, 2)[None],
+        query_gain[None],
+        key_gain[None],
         mix_lambda,
         head_gain[None],
         conv_taps,
     )
-    return result[None]
+    return (mine.astype(jnp.float32) + take.astype(jnp.float32)).astype(bf16)[None]
 
 
 def per_device(

time: 171 us -> 164 us (0.959)
  Pallas kernels: 166 us -> 161 us
  local copies, waits for them, and re-layouts: 4.24 us -> 0 us
  other arithmetic: 0 us -> 2.91 us
    pallas_call x1, Pallas kernels: 166 us -> 161 us  [split_device(): pl.pallas_call(lambda *refs: fused_kernel(n, half, *refs), out_shape=(jax...]
    unnamed x5 -> x0, local copies, waits for them, and re-layouts: 3.02 us -> none
    broadcast_in_dim x0 -> x1, other arithmetic: none -> 2.91 us  [split_device(): (mine.astype(jnp.float32) + take.astype(jnp.float32)).astype(bf16)[None]]
where the time goes in v2:
time: 164 us
  Pallas kernels  161 us (98%)
  other arithmetic  2.91 us (2%)
    pallas_call x1, Pallas kernels, split_device(): pl.pallas_call(lambda *refs: fused_kernel(n, half, *refs), out_shape=(jax...  161 us

profile of v2, /device:TPU:0, one launch (start us, length us, event | category | flops | bytes accessed | tf_op | source)
XLA Modules:
  0.0 163.7 jit_solution(12780435833767966344)
XLA Ops:
  0.0 160.8 %shard_map.145 = (bf16[256,2048]{1,0:T(8,128)(2,1)}, bf16[256,2048]{1,0:T(8,128)(2,1)}) custom-call(bf16[512,1024]{1,0:T(8,128)(2,1)} %bitcast.7, bf16[128,512]{1,0:T(8,128)(2,1)} %refs_1_.1, bf16[128,512]{1,0:T(8,128)(2,1)} %refs_2_.1, bf16[128,512]{1,0:T(8,128)(2,1)} %refs_3_.1, bf16[128,1024]{1,0:T(8,128)(2,1)} %refs_4_.1, bf16[128,1024]{1,0:T(8,128)(2,1)} %refs_5_.1, ...), custom_call_target="tpu_custom_call" | custom-call | tf_op jit(solution)/shard_map/pallas_call | solution.py:618
  160.8 2.9 %fusion = bf16[1,256,2048]{2,1,0:T(8,128)(2,1)} fusion(bf16[256,2048]{1,0:T(8,128)(2,1)} %get-tuple-element.8, bf16[256,2048]{1,0:T(8,128)(2,1)} %get-tuple-element.7), kind=kLoop, calls=%fused_computation.1 | loop fusion | flops 2097152 | bytes 3145728 | tf_op jit(solution)/shard_map/broadcast_in_dim | solution.py:665

commit v3 on v2

--- a/solution.py
+++ b/solution.py
@@ -134,7 +134,7 @@
     n, half, tok_ref, q_ref, k_ref, v_ref, post_ref, pre_ref, inner_ref, ao_ref, co_ref,
     ng_any, qg_any, kg_any, lam_ref, hg_any, taps_any, mine, take,
     gain_ref, qg_ref, kg_ref, hg_ref, taps_ref, acc, pack, w_all, t_raw, t_twin, t_all, o_raw, wo_all, query, key, val, post, signal, conv_hid,
-    attn_hid, hin, both,
+    attn_hid, hin, both, part_peak, part_total, part_sum,
     l_sem, z_send, z_recv, f_send, f_recv, g_send, g_recv, r_send, r_recv, t_send, t_recv,
     p_send, p_recv, o_send, o_recv, of_send, of_recv, og_send, og_recv, c_send, c_recv,
     a_send, a_recv, e_send, e_recv, s_sem,
@@ -279,11 +279,14 @@
             {"fs": (beside, above)[i]},
         )
 
-    def o_further(s, d):
-        held, to = (beside, above) if d % 2 == 0 else (above, beside)
-        return remote(
-            o_place(s, held), o_place(s, held), og_send.at[s], og_recv.at[s], {"fs": to}
-        )
+    def o_further(s, part):
+        held, to = (beside, above) if part == 0 else (above, beside)
+        at, size = s * fs + held, wo_all.shape[1] // 2
+        block = wo_all.at[
+            at // 2, pl.ds(part * size, size),
+            pl.ds(pl.multiple_of(at % 2 * w_rows, w_rows), w_rows),
+        ]
+        return remote(block, block, og_send.at[part, s], og_recv.at[part, s], {"fs": to})
 
     def both_ways(along):
         for step in (1, -1):
@@ -335,9 +338,9 @@
             o_side(s, i).start()
 
     def o_pass(at, s):
-        d = (at - s) % n
-        o_side(s, d % 2).wait_recv()
-        o_further(s, d).start()
+        for part in range(2):
+            o_side(s, part).wait_recv()
+            o_further(s, part).start()
 
     plans = []
     for at in range(n):
@@ -352,7 +355,8 @@
                 if visit + len(ring) < n:
                     events += [(o_event, r) for r in ring]
                     o_done += ring
-            plan.append(events + [(o_pass, r) for r in held])
+            passes = [(o_pass, r) for r in held]
+            plan.append(passes + events if visit == n - 1 else events + passes)
             passed += held
         plan.append([(o_event, r) for r in order[at] if r not in o_done])
         plan.append([(o_pass, r) for r in order[at] if r not in passed])
@@ -461,43 +465,107 @@
                 def _(s=s):
                     act(s)
 
+    a_rows = math.gcd(rows, 256)
+    each = rows // a_rows
+    scale = half ** (-0.5) * math.log2(math.e)
+    lam = lam_ref[place]
+    is_end = jnp.logical_or(z == 0, z == n - 1)
+    final = choose([order[at][n - 1] for at in range(n)], z)
+
+    def compare(which, at, keys):
+        return lax.dot_general(
+            query[which, at, :], key[keys, :], (((1,), (1,)), ((), ())),
+            preferred_element_type=f32,
+        ) * scale
+
+    def soft(which, at, keys):
+        scores = compare(which, at, keys)
+        peak = jnp.max(scores, axis=-1, keepdims=True)
+        expo = jnp.exp2(scores - peak)
+        total = jnp.sum(expo, axis=-1, keepdims=True)
+        return peak, total, jnp.dot(
+            expo.astype(bf16), val[keys, :], preferred_element_type=f32
+        )
+
+    def attend_first():
+        start = jnp.where(final == 0, rows, 0)
+        keys = pl.ds(pl.multiple_of(start, rows), total_rows - rows)
+
+        def some(i, unused):
+            at = pl.ds(pl.multiple_of(start + i * a_rows, a_rows), a_rows)
+            for which in range(2):
+                peak, total, accum = soft(which, at, keys)
+                part_peak[which, at, :] = peak
+                part_total[which, at, :] = total
+                part_sum[which, at, :] = accum
+            return unused
+
+        lax.fori_loop(0, (n - 1) * each, some, 0)
+
     project(z)
     for visit in range(1, n):
+        if visit == n - 1:
+            pl.when(is_end)(attend_first)
         follow(lambda at: plans[at][visit - 1])
         s = choose([order[at][visit] for at in range(n)], z)
         t_aside(s).wait_recv()
         project(s)
         each_whole(visit, convolve)
-        each_whole(visit, convolve_send)
+
+        @pl.when(is_end)
+        def _(visit=visit):
+            each_whole(visit, convolve_send)
     hin[:, conv_at] = conv_hid[own, :]
+    pl.when(jnp.logical_not(is_end))(attend_first)
     far = near[::-1]
 
-    a_rows = math.gcd(rows, 256)
-    each = rows // a_rows
-    scale = half ** (-0.5) * math.log2(math.e)
-    lam = lam_ref[place]
+    follow_rest = [lambda at, k=k: plans[at][n - 1 + k] for k in range(2)]
 
     def attend(i, unused):
-        for k, when in enumerate((0, (n * each) // 2 + 1)):
-            @pl.when(i == when)
-            def _(k=k):
-                follow(lambda at: plans[at][n - 1 + k])
-
-        d = choose(far + [0], i // each)
-        at = pl.ds(pl.multiple_of(((z + d) % n) * rows + (i % each) * a_rows, a_rows), a_rows)
-        maps = []
-        for which in range(2):
-            scores = lax.dot_general(
-                query[which, at, :], key[...], (((1,), (1,)), ((), ())),
-                preferred_element_type=f32,
-            ) * scale
-            expo = jnp.exp2(scores - jnp.max(scores, axis=-1, keepdims=True))
-            total = jnp.sum(expo, axis=-1, keepdims=True)
-            maps.append(
-                jnp.dot(expo.astype(bf16), val[...], preferred_element_type=f32) / total
-            )
-        head_out = maps[0] - lam * maps[1]
-        attn_hid[at, :] = scale_rows(head_out, hg_ref[...]).astype(bf16)
+        @pl.when(i == jnp.where(is_end, (n * each) // 2, 0))
+        def _():
+            follow(follow_rest[0])
+
+            @pl.when(jnp.logical_not(is_end))
+            def _():
+                for visit in range(1, n):
+                    each_whole(visit, convolve_send)
+
+        @pl.when(jnp.logical_and(i == n * each - 2, jnp.logical_not(is_end)))
+        def _():
+            follow(follow_rest[1])
+
+        block = (z + choose(far + [0], i // each)) % n
+        at = pl.ds(pl.multiple_of(block * rows + (i % each) * a_rows, a_rows), a_rows)
+
+        def finish(maps):
+            head_out = maps[0] - lam * maps[1]
+            attn_hid[at, :] = scale_rows(head_out, hg_ref[...]).astype(bf16)
+
+        @pl.when(block != final)
+        def _():
+            maps = []
+            late = pl.ds(pl.multiple_of(final * rows, rows), rows)
+            for which in range(2):
+                scores = compare(which, at, late)
+                before = part_peak[which, at, :]
+                peak = jnp.maximum(before, jnp.max(scores, axis=-1, keepdims=True))
+                factor, expo = jnp.exp2(before - peak), jnp.exp2(scores - peak)
+                total = part_total[which, at, :] * factor + jnp.sum(expo, axis=-1, keepdims=True)
+                accum = part_sum[which, at, :] * factor + jnp.dot(
+                    expo.astype(bf16), val[late, :], preferred_element_type=f32
+                )
+                maps.append(accum / total)
+            finish(maps)
+
+        @pl.when(block == final)
+        def _():
+            maps = []
+            for which in range(2):
+                unused_peak, total, accum = soft(which, at, pl.ds(0, total_rows))
+                maps.append(accum / total)
+            finish(maps)
+
         for j, d in enumerate(far):
             @pl.when(i == (j + 1) * each - 1)
             def _(d=d):
@@ -505,6 +573,11 @@
         return unused
 
     lax.fori_loop(0, n * each, attend, 0)
+
+    @pl.when(is_end)
+    def _():
+        follow(follow_rest[1])
+
     hin[:, attn_at] = attn_hid[own, :]
 
     def arrived(source, columns, d, send, recv):
@@ -539,11 +612,8 @@
 
     for visit in range(n):
         s = choose([order[at][visit] for at in range(n)], z)
-        for i in range(2):
-            @pl.when((z + n - s) % 2 != i)
-            def _(s=s, i=i):
-                o_side(s, i).wait_recv()
-        o_further(s, 0).wait_recv()
+        for part in range(2):
+            o_further(s, part).wait_recv()
         lax.fori_loop(s * (fs // 2), (s + 1) * (fs // 2), channel_part, 0)
     for d in near:
         arrived(attn_hid, attn_at, d, a_send, a_recv)
@@ -572,7 +642,7 @@
     for s in range(n):
         for i in range(2):
             o_side(s, i).wait_send()
-        o_further(s, 0).wait_send()
+            o_further(s, i).wait_send()
         for step in (1, -1):
             arrives = s <= z if step == 1 else s >= z
             @pl.when(jnp.logical_and(arrives, jnp.logical_and(z + step >= 0, z + step < n)))
@@ -643,10 +713,13 @@
             pltpu.VMEM((total, vsize), bf16),
             pltpu.VMEM((rows, hidden), bf16),
             pltpu.VMEM((pairs, rows, 2 * w_rows), bf16),
+            pltpu.VMEM((2, total, 1), jnp.float32),
+            pltpu.VMEM((2, total, 1), jnp.float32),
+            pltpu.VMEM((2, total, vsize), jnp.float32),
             dma((n * 6 + 8,)),
             dma((n,)), dma((n,)), dma((2, n)), dma((2, n)), dma((n,)), dma((n,)),
             dma((1,)), dma((1,)), dma((2, n)), dma((n,)), dma((n,)), dma((n,)),
-            dma((2, n)), dma((n,)), dma((2, n)), dma((2, n)), dma((n,)), dma((n,)),
+            dma((2, n)), dma((n,)), dma((2, n)), dma((2, n)), dma((2, n)), dma((2, n)),
             dma((n,)), dma((n,)), dma((n,)), dma((n,)), dma((pairs,)), dma((pairs,)), dma((pairs,)),
         ],
         compiler_params=pltpu.CompilerParams(

time: 164 us -> 155 us (0.945)
  Pallas kernels: 161 us -> 152 us
    pallas_call x1, Pallas kernels: 161 us -> 152 us  [split_device(): pl.pallas_call(lambda *refs: fused_kernel(n, half, *refs), out_shape=(jax...]
where the time goes in v3:
time: 155 us
  Pallas kernels  152 us (98%)
  other arithmetic  2.91 us (2%)
    pallas_call x1, Pallas kernels, split_device(): pl.pallas_call(lambda *refs: fused_kernel(n, half, *refs), out_shape=(jax...  152 us

profile of v3, /device:TPU:0, one launch (start us, length us, event | category | flops | bytes accessed | tf_op | source)
XLA Modules:
  0.0 154.8 jit_solution(15482344429910297916)
XLA Ops:
  0.0 151.9 %shard_map.145 = (bf16[256,2048]{1,0:T(8,128)(2,1)}, bf16[256,2048]{1,0:T(8,128)(2,1)}) custom-call(bf16[512,1024]{1,0:T(8,128)(2,1)} %bitcast.7, bf16[128,512]{1,0:T(8,128)(2,1)} %refs_1_.1, bf16[128,512]{1,0:T(8,128)(2,1)} %refs_2_.1, bf16[128,512]{1,0:T(8,128)(2,1)} %refs_3_.1, bf16[128,1024]{1,0:T(8,128)(2,1)} %refs_4_.1, bf16[128,1024]{1,0:T(8,128)(2,1)} %refs_5_.1, ...), custom_call_target="tpu_custom_call" | custom-call | tf_op jit(solution)/shard_map/pallas_call | solution.py:688
  151.9 2.9 %fusion = bf16[1,256,2048]{2,1,0:T(8,128)(2,1)} fusion(bf16[256,2048]{1,0:T(8,128)(2,1)} %get-tuple-element.8, bf16[256,2048]{1,0:T(8,128)(2,1)} %get-tuple-element.7), kind=kLoop, calls=%fused_computation.1 | loop fusion | flops 2097152 | bytes 3145728 | tf_op jit(solution)/shard_map/broadcast_in_dim | solution.py:738

commit v4 on v3

--- a/solution.py
+++ b/solution.py
@@ -526,10 +526,11 @@
         def _():
             follow(follow_rest[0])
 
-            @pl.when(jnp.logical_not(is_end))
-            def _():
-                for visit in range(1, n):
-                    each_whole(visit, convolve_send)
+
+        @pl.when(jnp.logical_and(i == each, jnp.logical_not(is_end)))
+        def _():
+            for visit in range(1, n):
+                each_whole(visit, convolve_send)
 
         @pl.when(jnp.logical_and(i == n * each - 2, jnp.logical_not(is_end)))
         def _():

time: 155 us -> 153 us (0.987)
  Pallas kernels: 152 us -> 150 us
    pallas_call x1, Pallas kernels: 152 us -> 150 us  [split_device(): pl.pallas_call(lambda *refs: fused_kernel(n, half, *refs), out_shape=(jax...]
where the time goes in v4:
time: 153 us
  Pallas kernels  150 us (98%)
  other arithmetic  2.91 us (2%)
    pallas_call x1, Pallas kernels, split_device(): pl.pallas_call(lambda *refs: fused_kernel(n, half, *refs), out_shape=(jax...  150 us

profile of v4, /device:TPU:0, one launch (start us, length us, event | category | flops | bytes accessed | tf_op | source)
XLA Modules:
  0.0 152.9 jit_solution(9139461305472688654)
XLA Ops:
  0.0 150.0 %shard_map.145 = (bf16[256,2048]{1,0:T(8,128)(2,1)}, bf16[256,2048]{1,0:T(8,128)(2,1)}) custom-call(bf16[512,1024]{1,0:T(8,128)(2,1)} %bitcast.7, bf16[128,512]{1,0:T(8,128)(2,1)} %refs_1_.1, bf16[128,512]{1,0:T(8,128)(2,1)} %refs_2_.1, bf16[128,512]{1,0:T(8,128)(2,1)} %refs_3_.1, bf16[128,1024]{1,0:T(8,128)(2,1)} %refs_4_.1, bf16[128,1024]{1,0:T(8,128)(2,1)} %refs_5_.1, ...), custom_call_target="tpu_custom_call" | custom-call | tf_op jit(solution)/shard_map/pallas_call | solution.py:689
  150.0 2.9 %fusion = bf16[1,256,2048]{2,1,0:T(8,128)(2,1)} fusion(bf16[256,2048]{1,0:T(8,128)(2,1)} %get-tuple-element.8, bf16[256,2048]{1,0:T(8,128)(2,1)} %get-tuple-element.7), kind=kLoop, calls=%fused_computation.1 | loop fusion | flops 2097152 | bytes 3145728 | tf_op jit(solution)/shard_map/broadcast_in_dim | solution.py:739
